TPU v7x, 32 devices: a whole 2x2x4 slice. The times are simulated.
32 devices in a mesh: sp: 8 (over z, y), tp: 4 (over x, core).
Axes of the slice: x: 2, y: 2, z: 4, core: 2. Of those that a mesh axis runs over, the one named last changes fastest.
Arguments:
- memory_queries: bfloat16 [4096, 1024], P('sp', 'tp'), may hold values from -8 to 8
- memory_keys: bfloat16 [4096, 1024], P('sp', 'tp'), may hold values from -8 to 8
- memory_values: bfloat16 [4096, 1024], P('sp', 'tp'), may hold values from -6 to 6
- input_gate_logits: float32 [8, 4096], P('tp', 'sp'), may hold values from -64 to 160
- forget_gate_logits: float32 [8, 4096], P('tp', 'sp'), may hold values from -0.1 to 20
- extra_log_decay: float32 [8, 4096], P('tp', 'sp'), may hold values from -1.4 to 0
- residual: bfloat16 [4096, 2048], P(('sp', 'tp')), may hold values from -6 to 6
- cell_output_weight: bfloat16 [1024, 2048], P('tp', 'sp'), may hold values from -0.1875 to 0.1875
- expert_norm_gain: float32 [2048], replicated, may hold values from 0.1 to 1.9
- expert_gate_weight: bfloat16 [8, 2048, 3584], P('sp', None, 'tp'), may hold values from -0.125 to 0.125
- expert_up_weight: bfloat16 [8, 2048, 3584], P('sp', None, 'tp'), may hold values from -0.125 to 0.125
- expert_down_weight: bfloat16 [8, 3584, 2048], P('sp', 'tp'), may hold values from -0.09375 to 0.09375
- routed_expert_index: int32 [4096, 2], P('sp'), may hold values from 0 to 7, as said below
- routed_expert_weight: float32 [4096, 2], P(('sp', 'tp')), may hold values from 0.1 to 1
Outputs:
- layer_out: bfloat16 [4096, 2048], P(('sp', 'tp'))
Inputs may be any that keep to these rules, and one draw needn't show every extreme that they name: `routed_expert_index`: each row names 2 different experts. In each aligned block of 128 rows (the rows of one device after the cell) no expert is named more than 40 times, and one expert is named exactly 40 times in every block.
All inputs are finite; a program needn't handle non-finite values.
Results may differ from a plain program's by a relative error of at most 0.013.
Values may be sent and summed in bfloat16 or wider, within the bound.
A program may use at most 128 MiB of HBM per device.

v0:
```python
import jax
import jax.numpy as jnp
from jax import lax
from jax.sharding import PartitionSpec as P

highest = lax.Precision.HIGHEST
lowest = -1e30
epsilon = 1e-06


def carried_in(x, axis, combine, identity):
    length, place = (lax.axis_size(axis), lax.axis_index(axis))
    everything = jax.tree.map(lambda part: lax.all_gather(part, axis), x)
    start = jax.tree.map(
        lambda part, zero: jnp.broadcast_to(jnp.asarray(zero, part.dtype), part.shape), x, identity
    )

    def turn(k, before):
        reached = k < place
        new = combine(before, jax.tree.map(lambda part: part[k], everything))
        return jax.tree.map(lambda a, b: jnp.where(reached, a, b), new, before)

    return lax.fori_loop(0, length, turn, start)


def block_pass(memory, inputs):
    state_mat, state_norm, state_max = memory
    queries, keys_blk, values_blk, gate_in, forget_log_value = inputs
    length = gate_in.shape[-1]
    running = jnp.cumsum(forget_log_value, axis=-1)
    causal = jnp.arange(length)[:, None] >= jnp.arange(length)[None, :]
    exponent = running[:, :, None] - running[:, None, :] + gate_in[:, None, :]
    exponent = jnp.where(causal[None], exponent, -jnp.inf)
    carried = running + state_max[:, None]
    row_max = jnp.maximum(carried, jnp.max(exponent, axis=-1))
    decays = jnp.exp(exponent - row_max[:, :, None])
    carry_scale = jnp.exp(carried - row_max)
    dispatch_affinity = jnp.einsum("htk,hsk->hts", queries, keys_blk, precision=highest) * decays
    numerator = carry_scale[:, :, None] * jnp.einsum(
        "hvk,htk->htv", state_mat, queries, precision=highest
    )
    numerator = numerator + jnp.einsum(
        "hts,hsv->htv", dispatch_affinity, values_blk, precision=highest
    )
    denominator = carry_scale * jnp.einsum(
        "hk,htk->ht", state_norm, queries, precision=highest
    ) + jnp.sum(dispatch_affinity, axis=-1)
    final_log = running[:, -1]
    log_prev = final_log + state_max
    log_keep = final_log[:, None] - running + gate_in
    new_max = jnp.maximum(log_prev, jnp.max(log_keep, axis=-1))
    prev_scale = jnp.exp(log_prev - new_max)
    retain = jnp.exp(log_keep - new_max[:, None])
    new_mat = prev_scale[:, None, None] * state_mat + jnp.einsum(
        "hsv,hsk->hvk", retain[:, :, None] * values_blk, keys_blk, precision=highest
    )
    new_norm = prev_scale[:, None] * state_norm + jnp.einsum(
        "hs,hsk->hk", retain, keys_blk, precision=highest
    )
    return ((new_mat, new_norm, new_max), (numerator, denominator, row_max))


def join_states(earlier, later):
    early_log, early_mat, early_norm, early_max = earlier
    late_log, late_mat, late_norm, late_max = later
    joined_max = jnp.maximum(early_max + late_log, late_max)
    early_scale = jnp.exp(early_max + late_log - joined_max)
    late_scale = jnp.exp(late_max - joined_max)
    joined_mat = early_scale[:, None, None] * early_mat + late_scale[:, None, None] * late_mat
    joined_norm = early_scale[:, None] * early_norm + late_scale[:, None] * late_norm
    return (early_log + late_log, joined_mat, joined_norm, joined_max)


def matrix_memory_step(
    memory_queries,
    memory_keys,
    memory_values,
    input_gate_logits,
    forget_gate_logits,
    extra_log_decay,
):
    tokens_here, channels = memory_queries.shape
    heads_here = input_gate_logits.shape[0]
    head_dim = channels // heads_here

    def heads_first(tensor):
        return jnp.transpose(
            tensor.astype(jnp.float32).reshape(tokens_here, heads_here, head_dim), (1, 0, 2)
        )

    queries = heads_first(memory_queries) * head_dim ** (-0.5)
    forget_log_value = jax.nn.log_sigmoid(forget_gate_logits) + extra_log_decay
    block_size = min(tokens_here, 256)
    block_count = tokens_here // block_size

    def split_blocks(tensor):
        return jnp.moveaxis(
            tensor.reshape((heads_here, block_count, block_size) + tensor.shape[2:]), 1, 0
        )

    def join_blocks(tensor):
        return jnp.moveaxis(tensor, 0, 1).reshape((heads_here, tokens_here) + tensor.shape[3:])

    empty_state = (
        jnp.zeros((heads_here, head_dim, head_dim), jnp.float32),
        jnp.zeros((heads_here, head_dim), jnp.float32),
        jnp.full((heads_here,), lowest, jnp.float32),
    )
    members = (
        queries,
        heads_first(memory_keys),
        heads_first(memory_values),
        input_gate_logits,
        forget_log_value,
    )
    end_state, pieces = lax.scan(
        block_pass, empty_state, tuple((split_blocks(member) for member in members))
    )
    numerator, denominator, row_max = (join_blocks(member) for member in pieces)
    running = jnp.cumsum(forget_log_value, axis=-1)
    identity = (jnp.zeros((heads_here,), jnp.float32),) + empty_state
    incoming = carried_in((running[:, -1],) + tuple(end_state), "sp", join_states, identity)
    prior_mat, prior_norm, prior_max = incoming[1:]
    reached = running + prior_max[:, None]
    joined = jnp.maximum(row_max, reached)
    local_scale = jnp.exp(row_max - joined)
    carry_scale = jnp.exp(reached - joined)
    numerator = local_scale[:, :, None] * numerator + carry_scale[:, :, None] * jnp.einsum(
        "hvk,htk->htv", prior_mat, queries, precision=highest
    )
    denominator = local_scale * denominator + carry_scale * jnp.einsum(
        "hk,htk->ht", prior_norm, queries, precision=highest
    )
    guarded = jnp.maximum(jnp.abs(denominator), jnp.exp(-joined))
    return ((numerator / guarded[:, :, None]).astype(jnp.bfloat16), heads_here, head_dim)


def slot_index(ids, experts, capacity):
    flat_ids = ids.reshape(-1)
    matches = (flat_ids[:, None] == jnp.arange(experts, dtype=jnp.int32)[None, :]).astype(jnp.int32)
    before = jnp.cumsum(matches, axis=0) - matches
    return flat_ids * capacity + jnp.sum(before * matches, axis=1)


def local(
    memory_queries,
    memory_keys,
    memory_values,
    input_gate_logits,
    forget_gate_logits,
    extra_log_decay,
    residual,
    cell_output_weight,
    expert_norm_gain,
    expert_gate_weight,
    expert_up_weight,
    expert_down_weight,
    routed_expert_index,
    routed_expert_weight,
):
    hidden, heads_here, head_dim = matrix_memory_step(
        memory_queries,
        memory_keys,
        memory_values,
        input_gate_logits,
        forget_gate_logits,
        extra_log_decay,
    )
    weight_piece = lax.all_gather(cell_output_weight, "sp", axis=1, tiled=True)
    shaped = weight_piece.reshape(heads_here, head_dim, weight_piece.shape[1])
    partial_rows = jnp.einsum(
        "htd,hdc->tc", hidden, shaped, preferred_element_type=jnp.float32
    ).astype(jnp.bfloat16)
    projected = lax.psum_scatter(
        partial_rows.astype(jnp.float32).astype(jnp.bfloat16), "tp", scatter_dimension=0, tiled=True
    ).astype(jnp.float32)
    mixed_rows = (residual.astype(jnp.float32) + projected).astype(jnp.bfloat16)
    mixed_wide = mixed_rows.astype(jnp.float32)
    norm_scale = lax.rsqrt(jnp.mean(mixed_wide * mixed_wide, axis=-1, keepdims=True) + epsilon)
    normed = (mixed_wide * norm_scale * expert_norm_gain).astype(jnp.bfloat16)
    sp_size = lax.axis_size("sp")
    row_count, model_width = residual.shape
    top_count = routed_expert_index.shape[1]
    experts = sp_size * expert_gate_weight.shape[0]
    assigned = row_count * top_count
    capacity = max(2, assigned * 5 // (4 * experts))
    own_ids = lax.dynamic_slice_in_dim(
        routed_expert_index, lax.axis_index("tp") * row_count, row_count, 0
    )
    own_slots = slot_index(own_ids, experts, capacity)
    zero_row = jnp.zeros((1, model_width), jnp.bfloat16)
    padded = jnp.concatenate([normed, zero_row], axis=0)
    slot_table = jnp.full((experts * capacity,), row_count, jnp.int32)
    slot_table = slot_table.at[own_slots].set(jnp.arange(assigned, dtype=jnp.int32) // top_count)
    arrived = lax.all_gather(
        lax.all_to_all(
            padded[slot_table.reshape(experts, 1, capacity)],
            "sp",
            split_axis=0,
            concat_axis=0,
            tiled=True,
        ),
        "tp",
        axis=1,
        tiled=True,
    )
    sources, owners, slot_span, width_in = arrived.shape
    flat_rows = arrived.reshape(-1, width_in)
    gate_pre = jnp.dot(flat_rows, expert_gate_weight[0], preferred_element_type=jnp.float32)
    up_pre = jnp.dot(flat_rows, expert_up_weight[0], preferred_element_type=jnp.float32)
    hidden_act = (jax.nn.silu(gate_pre) * up_pre).astype(jnp.bfloat16)
    group_term = jnp.dot(hidden_act, expert_down_weight[0], preferred_element_type=jnp.float32)
    group_term = lax.optimization_barrier(group_term.astype(jnp.bfloat16)).astype(jnp.float32)
    summed = lax.psum_scatter(
        group_term.reshape(sources, owners, slot_span, width_in).astype(jnp.bfloat16),
        "tp",
        scatter_dimension=1,
        tiled=True,
    )
    returned = lax.all_to_all(summed, "sp", split_axis=0, concat_axis=0, tiled=True)
    picked = returned.reshape(experts * capacity, model_width)[own_slots]
    picked = picked.reshape(row_count, top_count, model_width).astype(jnp.float32)
    routed_sum = jnp.sum(picked * routed_expert_weight[:, :, None], axis=1)
    return (mixed_wide + routed_sum).astype(jnp.bfloat16)


def solution(mesh):
    return jax.shard_map(
        local,
        mesh=mesh,
        in_specs=(
            P("sp", "tp"),
            P("sp", "tp"),
            P("sp", "tp"),
            P("tp", "sp"),
            P("tp", "sp"),
            P("tp", "sp"),
            P(("sp", "tp"), None),
            P("tp", "sp"),
            P(),
            P("sp", None, "tp"),
            P("sp", None, "tp"),
            P("sp", "tp", None),
            P("sp", None),
            P(("sp", "tp"), None),
        ),
        out_specs=P(("sp", "tp"), None),
        check_vma=False,
    )
```

profile of v0, /device:TPU:0, one launch (start us, length us, event | category | flops | bytes accessed | tf_op | source)
XLA Modules:
  0.0 404.9 jit_solution(8255470432722626242)
XLA Ops:
  6.6 1.1 copy.56
  7.8 0.2 copy.57
  8.0 1.1 copy.54
  9.9 11.3 %while.39 = (s32[]{:T(128)}, f32[2,128,128]{2,1,0:T(8,128)S(1)}, f32[2,128]{1,0:T(2,128)S(1)}, f32[2]{0:T(128)S(1)}, f32[2,2,256,128]{3,2,0,1:T(8,128)S(1)}, /*i...) while((s32[]{:T(128)}, f32[2,128,128]{2,1,0:T(8,128)S(1)}, ...), condition=%wide.region_6.7_spmd.clone, body=%wide.region_0.6_spmd.clone.sunk | while | flops 607329536 | bytes 4625314 | solution.py:116
  9.9 0.6 reduce-window.38
  11.4 0.2 fusion.122
  11.7 0.6 fusion.123
  12.4 0.2 fusion.121
  12.7 0.3 fusion.124
  13.3 0.4 convolution_multiply_fusion.4
  13.6 1.0 fusion.125
  14.8 0.7 convolution_add_fusion.3
  15.6 0.6 reduce-window.38
  17.0 0.2 fusion.122
  17.3 0.6 fusion.123
  18.0 0.2 fusion.121
  18.4 0.3 fusion.124
  18.9 0.4 convolution_multiply_fusion.4
  19.3 1.0 fusion.125
  20.4 0.7 convolution_add_fusion.3
  21.2 0.6 copy-done
  21.9 0.7 all-gather.9.cloned.1.call-update
  22.7 0.6 reduce-window.22
  23.9 0.7 dynamic-slice
  25.3 0.2 dynamic-update-slice.1
  25.6 23.2 %all-reduce.4 = (f32[16]{0:T(128)S(1)}, f32[16]{0:T(128)S(1)}) all-reduce(f32[16]{0:T(128)S(1)} %bitcast_dynamic-update-slice_fusion.1, f32[16]{0:T(128)S(1)} %dynamic-update-slice.1), channel_id=2, replica_groups=mesh['sp'=8,'tp'=4] {'sp'}, use_global_device_ids=true, to_apply=%add.1 | all-reduce | flops 32 | bytes 256
  49.0 16.4 %all-gather.4 = f32[8,2,128]{2,1,0:T(2,128)S(1)} all-gather(f32[1,2,128]{2,1,0:T(2,128)S(1)} %bitcast.293), channel_id=5, replica_groups=mesh['sp'=8,'tp'=4] {'sp'}, dimensions={0}, use_global_device_ids=true | all-gather | bytes 9216 | tf_op jit(solution)/shard_map/all_gather | solution.py:13
  65.4 9.0 %while.40 = (s32[]{:T(128)}, f32[2,128,128]{2,1,0:T(8,128)S(1)}, f32[2,128]{1,0:T(2,128)S(1)}, f32[2]{0:T(128)S(1)}, s32[]{:T(128)}, /*index=5*/f32[8,2]{1,0:T(8...) while((s32[]{:T(128)}, f32[2,128,128]{2,1,0:T(8,128)S(1)}, ...), condition=%wide.region_10.11_spmd.clone, body=%wide.region_9.10_spmd.clone.sunk | while | flops 165138 | bytes 396541 | solution.py:23
  65.5 1.0 fusion.126
  66.6 1.0 fusion.126
  67.7 1.0 fusion.126
  68.8 1.0 fusion.126
  69.9 1.0 fusion.126
  71.1 1.0 fusion.126
  72.2 1.0 fusion.126
  73.3 1.0 fusion.126
  74.4 0.4 fusion.66
  74.9 0.2 bitcast_multiply_fusion.5
  75.1 1.2 fusion.47
  76.3 29.1 %all-gather.9.cloned.1.call-done = bf16[256,2048]{1,0:T(8,128)(2,1)} async-done(((bf16[256,256]{1,0:T(8,128)(2,1)}), bf16[256,2048]{1,0:T(8,128)(2,1)}) %all-gather.9.cloned.1.call-update) | async-done | bytes 1048592 | tf_op jit(solution)/shard_map/all_gather | solution.py:169
  105.3 3.3 bitcast_convert_fusion
  108.7 0.7 broadcast_multiply_fusion
  109.8 0.6 reduce-window.26
  110.4 0.2 slice_reduce_fusion.2
  111.0 1.4 scatter_custom_fusion
  112.6 26.4 %reduce-scatter.3.cloned.1.call-done = bf16[128,2048]{1,0:T(8,128)(2,1)} async-done(((bf16[512,2048]{1,0:T(8,128)(2,1)}), bf16[128,2048]{1,0:T(8,128)(2,1)}) %reduce-scatter.3.cloned.1.call-update) | async-done | bytes 524304 | tf_op jit(solution)/shard_map/reduce_scatter | solution.py:174
  139.0 1.3 fusion.48
  140.3 1.3 fusion.50
  141.6 2.4 gather_fusion
  144.0 36.6 %all_to_all.10 = bf16[8,1,40,2048]{3,2,1,0:T(8,128)(2,1)} all-to-all(bf16[8,1,40,2048]{3,2,1,0:T(8,128)(2,1)S(1)} %bitcast.275), channel_id=1, replica_groups=mesh['sp'=8,'tp'=4] {'sp'}, dimensions={0} | all-to-all | bytes 2621440 | tf_op jit(solution)/shard_map/all_to_all | solution.py:196
  180.7 0.2 all-reduce.7.cloned.1.call-start
  180.9 38.4 %all-gather.11.cloned.1.call-done = bf16[8,4,40,2048]{3,2,1,0:T(8,128)(2,1)} async-done(((bf16[8,1,40,2048]{3,2,1,0:T(8,128)(2,1)}), bf16[8,4,40,2048]{3,2,1,0:T(8,128)(2,1)}) %all-gather.11.cloned.1.call-update) | async-done | bytes 5242896 | tf_op jit(solution)/shard_map/all_gather | solution.py:195
  219.3 10.0 %fusion.43 = f32[1280,896]{1,0:T(8,128)} fusion(bf16[1280,2048]{1,0:T(8,128)(2,1)} %bitcast.302, bf16[1,2048,896]{2,1,0:T(8,128)(2,1)} %param.27), kind=kOutput, calls=%fused_computation.81 | convolution fusion | flops 4697620480 | bytes 13500416 | tf_op jit(solution)/shard_map/dot_general | solution.py:209
  229.3 17.6 %convolution_convert_fusion = bf16[1280,2048]{1,0:T(8,128)(2,1)} fusion(bf16[1,896,2048]{2,1,0:T(8,128)(2,1)} %param.29, f32[1280,896]{1,0:T(8,128)} %fusion.43, bf16[1280,2048]{1,0:T(8,128)(2,1)} %bitcast.303, bf16[1,2048,896]{2,1,0:T(8,128)(2,1)} %param.28), kind=kOutput, calls=%fused_computation.76 | convolution fusion | flops 9404743680 | bytes 22413312 | tf_op jit(solution)/shard_map/dot_general | solution.py:212
  246.9 0.6 copy-done.9
  247.5 0.6 dynamic-slice.2
  248.1 101.5 %all-reduce.7.cloned.1.call-done = bf16[8,4,40,2048]{3,2,1,0:T(8,128)(2,1)} async-done(((bf16[8,4,40,2048]{3,2,1,0:T(8,128)(2,1)}), bf16[8,4,40,2048]{3,2,1,0:T(8,128)(2,1)}) %all-reduce.7.cloned.1.call-update) | async-done | bytes 5242896
  349.6 3.2 constant_dynamic-slice_fusion.3
  352.8 5.5 %all-to-all-start.1 = ((bf16[8,1,40,2048]{3,2,1,0:T(8,128)(2,1)}), bf16[8,1,40,2048]{3,2,1,0:T(8,128)(2,1)S(1)}, u32[]{:S(2)}, u32[]{:S(2)}) async-start(bf16[8,1,40,2048]{3,2,1,0:T(8,128)(2,1)} %constant_dynamic-slice_fusion.3), calls=%async_computation.2 | async-start | bytes 2621440 | tf_op jit(solution)/shard_map/all_to_all | solution.py:220
  358.5 30.9 %all-to-all-done.1 = bf16[8,1,40,2048]{3,2,1,0:T(8,128)(2,1)S(1)} async-done(((bf16[8,1,40,2048]{3,2,1,0:T(8,128)(2,1)}), bf16[8,1,40,2048]{3,2,1,0:T(8,128)(2,1)S(1)}, u32[]{:S(2)}, u32[]{:S(2)}) %all-to-all-start.1) | async-done | bytes 1310752 | tf_op jit(solution)/shard_map/all_to_all | solution.py:220
  389.4 2.3 gather_fusion.1
  391.7 2.4 reshape.428
  394.2 3.2 multiply_reduce_fusion
  397.3 1.0 fusion.51
  (137 shorter events, 6.6 us)
Async XLA Ops:
  6.5 2.9 copy-start.3
  6.5 3.3 copy-start.7
  6.5 3.3 copy-start.6
  6.5 3.3 copy-start.4
  6.5 58.9 %all-gather.13.cloned.1.call-start = ((), (), s32[]{:S(2)}) async-start(), calls=%async_computation.6 | async-start | bytes 1179648 | tf_op jit(solution)/shard_map/all_gather | solution.py:13
  9.9 14.0 %copy-start.10 = (u32[32]{0:T(128)S(1)}, u32[32]{0:T(128)}, u32[]{:S(2)}) copy-start(u32[32]{0:T(128)} %constant.125) | copy-start | bytes 388
  21.2 0.7 copy-start
  21.8 83.5 %all-gather.9.cloned.1.call-start = ((), (), s32[]{:S(2)}) async-start(), calls=%async_computation.3 | async-start | bytes 1179648 | tf_op jit(solution)/shard_map/all_gather | solution.py:169
  22.6 116.4 %reduce-scatter.3.cloned.1.call-start = ((), (), s32[]{:S(2)}) async-start(), calls=%async_computation.4 | async-start | bytes 2621440 | tf_op jit(solution)/shard_map/reduce_scatter | solution.py:174
  75.1 63.9 %copy-start.1 = (bf16[128,2048]{1,0:T(8,128)(2,1)S(1)}, bf16[128,2048]{1,0:T(8,128)(2,1)}, u32[]{:S(2)}) copy-start(bf16[128,2048]{1,0:T(8,128)(2,1)} %param.24) | copy-start | bytes 1572868
  76.2 64.0 %copy-start.5 = (f32[2048]{0:T(1024)S(1)}, f32[2048]{0:T(1024)}, u32[]{:S(2)}) copy-start(f32[2048]{0:T(1024)} %param.26) | copy-start | bytes 24580
  108.6 110.7 %all-gather.11.cloned.1.call-start = ((), (), s32[]{:S(2)}) async-start(), calls=%async_computation.5 | async-start | bytes 6553600 | tf_op jit(solution)/shard_map/all_gather | solution.py:195
  180.7 168.9 %all-reduce.7.cloned.1.call-start = ((), (), s32[]{:S(2)}) async-start(), calls=%async_computation.7 | async-start | bytes 10485760
  246.9 0.7 copy-start.9
  246.9 111.4 %copy-start.8 = (f32[128,2]{0,1:T(2,128)S(1)}, f32[128,2]{0,1:T(2,128)}, u32[]{:S(2)}) copy-start(f32[128,2]{0,1:T(2,128)} %param.31) | copy-start | bytes 3076
  352.8 36.5 %all-to-all-start.1 = ((bf16[8,1,40,2048]{3,2,1,0:T(8,128)(2,1)}), bf16[8,1,40,2048]{3,2,1,0:T(8,128)(2,1)S(1)}, u32[]{:S(2)}, u32[]{:S(2)}) async-start(bf16[8,1,40,2048]{3,2,1,0:T(8,128)(2,1)} %constant_dynamic-slice_fusion.3), calls=%async_computation.2 | async-start | bytes 2621440 | tf_op jit(solution)/shard_map/all_to_all | solution.py:220
  391.7 5.6 %copy-start.2 = (bf16[128,2048]{1,0:T(8,128)(2,1)S(1)}, bf16[128,2048]{1,0:T(8,128)(2,1)}, u32[]{:S(2)}) copy-start(bf16[128,2048]{1,0:T(8,128)(2,1)} %reduce-scatter.3.cloned.1.call-done) | copy-start | bytes 1572868
Sparse Core Ops, SparseCore 0:
  22.0 43.1 all-gather.12
  67.2 38.0 all-gather.8
  108.8 30.1 reduce-scatter.2
  180.8 38.4 all-gather.10
  247.0 102.5 all-reduce.6
where the time goes:
time: 406 us; the launch traced here: 405 us
  waiting for transfers between devices  227 us (56%)
  blocking collectives  76.3 us (19%)
  matrix products  39.1 us (10%)
  other arithmetic  22 us (5%)
  local copies, waits for them, and re-layouts  20.1 us (5%)
  between operations  14.2 us (3%)
  starting transfers between devices  5.89 us (1%)
    unnamed x6, waiting for transfers between devices  102 us
    all_gather x1, waiting for transfers between devices, local(): lax.all_gather(lax.all_to_all(padded[slot_table.reshape(experts, 1, capac...  38.4 us
    all_to_all x1, blocking collectives, local(): lax.all_to_all(padded[slot_table.reshape(experts, 1, capacity)], 'sp', sp...  36.6 us
    all_to_all x1, waiting for transfers between devices, local(): lax.all_to_all(summed, 'sp', split_axis=0, concat_axis=0, tiled=True)  30.9 us
    all_gather x1, waiting for transfers between devices, local(): weight_piece = lax.all_gather(cell_output_weight, 'sp', axis=1, tiled=True)  29.1 us
    reduce_scatter x1, waiting for transfers between devices, local(): lax.psum_scatter(partial_rows.astype(jnp.float32).astype(jnp.bfloat16), '...  26.4 us
    unnamed x1, blocking collectives  23.2 us
    dot_general x1, matrix products, local(): jnp.dot(hidden_act, expert_down_weight[0], preferred_element_type=jnp.flo...  17.6 us
  transfers between devices with their start and end apart: 6, of which 5 were waited for; matrix products, arithmetic and copies ran while one was open for 4% of the time, Pallas kernels for 0%

commit v1 on v0

--- a/solution.py
+++ b/solution.py
@@ -1,6 +1,9 @@
+import functools
 import jax
 import jax.numpy as jnp
 from jax import lax
+from jax.experimental import pallas as pl
+from jax.experimental.pallas import tpu as pltpu
 from jax.sharding import PartitionSpec as P
 
 highest = lax.Precision.HIGHEST
@@ -8,19 +11,238 @@
 epsilon = 1e-06
 
 
-def carried_in(x, axis, combine, identity):
-    length, place = (lax.axis_size(axis), lax.axis_index(axis))
-    everything = jax.tree.map(lambda part: lax.all_gather(part, axis), x)
-    start = jax.tree.map(
-        lambda part, zero: jnp.broadcast_to(jnp.asarray(zero, part.dtype), part.shape), x, identity
-    )
-
-    def turn(k, before):
-        reached = k < place
-        new = combine(before, jax.tree.map(lambda part: part[k], everything))
-        return jax.tree.map(lambda a, b: jnp.where(reached, a, b), new, before)
-
-    return lax.fori_loop(0, length, turn, start)
+def places():
+    sp, tp = lax.axis_index("sp"), lax.axis_index("tp")
+    n = lax.axis_size("sp")
+    return sp, tp, n, tp + 1 - 2 * (tp % 2), (tp + 2) % 4
+
+
+def greet(devices):
+    barrier = pltpu.get_barrier_semaphore()
+    for device in devices:
+        pl.semaphore_signal(
+            barrier, inc=1, device_id=device, device_id_type=pl.DeviceIdType.MESH
+        )
+    pl.semaphore_wait(barrier, len(devices))
+
+
+def remote(src, dst, send, recv, device):
+    return pltpu.make_async_remote_copy(
+        src_ref=src,
+        dst_ref=dst,
+        send_sem=send,
+        recv_sem=recv,
+        device_id=device,
+        device_id_type=pl.DeviceIdType.MESH,
+    )
+
+
+def dispatch_kernel(x_ref, out_ref, send_sems, recv_sems):
+    sp, tp, n, p, q = places()
+    peers = [((sp + k) % n, tp) for k in range(1, n)]
+    greet(peers + [(sp, p), (sp, q)])
+    started, across = [], []
+    first = [None]
+    for k in range(1, n):
+        copy = remote(
+            x_ref.at[(sp + k) % n], out_ref.at[tp, sp],
+            send_sems.at[0, k], recv_sems.at[0, k], peers[k - 1],
+        )
+        copy.start()
+        first.append(copy)
+    started += first[1:]
+    late = []
+
+    def relay(k):
+        across[k].wait_recv()
+        s = (sp - k + n) % n
+        copy = remote(
+            out_ref.at[q, s], out_ref.at[q, s], send_sems.at[3, k], recv_sems.at[3, k], (sp, p)
+        )
+        copy.start()
+        late.append(copy)
+
+    for k in range(n):
+        s = (sp - k + n) % n
+        if k == 0:
+            src = x_ref.at[sp]
+        else:
+            first[k].wait_recv()
+            src = out_ref.at[tp, s]
+        copy = remote(src, out_ref.at[tp, s], send_sems.at[1, k], recv_sems.at[1, k], (sp, q))
+        copy.start()
+        across.append(copy)
+        copy = remote(src, out_ref.at[tp, s], send_sems.at[2, k], recv_sems.at[2, k], (sp, p))
+        copy.start()
+        late.append(copy)
+        if k == 0:
+            out_ref[tp, sp] = x_ref[sp]
+        else:
+            relay(k - 1)
+    relay(n - 1)
+    for copy in late:
+        copy.wait()
+    for copy in started + across:
+        copy.wait_send()
+
+
+def dispatch(x):
+    n, rows, width = x.shape
+    return pl.pallas_call(
+        dispatch_kernel,
+        out_shape=jax.ShapeDtypeStruct((4, n, rows, width), x.dtype),
+        in_specs=[pl.BlockSpec(memory_space=pltpu.VMEM)],
+        out_specs=pl.BlockSpec(memory_space=pltpu.VMEM),
+        scratch_shapes=[pltpu.SemaphoreType.DMA((4, n)), pltpu.SemaphoreType.DMA((4, n))],
+        compiler_params=pltpu.CompilerParams(
+            collective_id=1, has_side_effects=True, vmem_limit_bytes=58 * 2**20
+        ),
+    )(x)
+
+
+def collect_kernel(back, x_ref, out_ref, near, sent, far, result, send_sems, recv_sems):
+    sp, tp, n, p, q = places()
+    chunks = x_ref.shape[1]
+    peers = [((sp + k) % n, tp) for k in range(1, n)] if back else []
+    greet(peers + [(sp, p), (sp, q)])
+
+    def at(k):
+        return (sp + 1 + k) % n if back else k
+
+    near_far, near_own, crossing, homeward = [], [], [], []
+    for k in range(chunks):
+        copy = remote(
+            x_ref.at[(p + 2) % 4, at(k)], near.at[0, k],
+            send_sems.at[0, k], recv_sems.at[0, k], (sp, p),
+        )
+        copy.start()
+        near_far.append(copy)
+    for k in range(chunks):
+        copy = remote(
+            x_ref.at[p, at(k)], near.at[1, k], send_sems.at[1, k], recv_sems.at[1, k], (sp, p)
+        )
+        copy.start()
+        near_own.append(copy)
+    for k in range(chunks):
+        near_far[k].wait_recv()
+        total = x_ref[q, at(k)].astype(jnp.float32) + near[0, k].astype(jnp.float32)
+        sent[k] = total.astype(jnp.bfloat16)
+        copy = remote(sent.at[k], far.at[k], send_sems.at[2, k], recv_sems.at[2, k], (sp, q))
+        copy.start()
+        crossing.append(copy)
+    for k in range(chunks):
+        near_own[k].wait_recv()
+        crossing[k].wait_recv()
+        total = x_ref[tp, at(k)].astype(jnp.float32) + near[1, k].astype(jnp.float32)
+        total = (total + far[k].astype(jnp.float32)).astype(jnp.bfloat16)
+        if not back:
+            out_ref[k] = total
+        elif k == chunks - 1:
+            out_ref[sp] = total
+        else:
+            result[k] = total
+            copy = remote(
+                result.at[k], out_ref.at[sp], send_sems.at[3, k], recv_sems.at[3, k], peers[k]
+            )
+            copy.start()
+            homeward.append(copy)
+    for copy in homeward:
+        copy.wait()
+    for copy in near_far + near_own + crossing:
+        copy.wait_send()
+
+
+def collect(x, back):
+    _, n, rows, width = x.shape
+    block = (n, rows, width)
+    return pl.pallas_call(
+        functools.partial(collect_kernel, back),
+        out_shape=jax.ShapeDtypeStruct(block, x.dtype),
+        in_specs=[pl.BlockSpec(memory_space=pltpu.VMEM)],
+        out_specs=pl.BlockSpec(memory_space=pltpu.VMEM),
+        scratch_shapes=[
+            pltpu.VMEM((2,) + block, x.dtype),
+            pltpu.VMEM(block, x.dtype),
+            pltpu.VMEM(block, x.dtype),
+            pltpu.VMEM(block if back else (1, 16, 128), x.dtype),
+            pltpu.SemaphoreType.DMA((4, n)),
+            pltpu.SemaphoreType.DMA((4, n)),
+        ],
+        compiler_params=pltpu.CompilerParams(
+            collective_id=2 if back else 3, has_side_effects=True, vmem_limit_bytes=58 * 2**20
+        ),
+    )(x)
+
+
+def spread_kernel(x_ref, out_ref, send_sems, recv_sems):
+    sp, tp, n, _, _ = places()
+    half = n // 2
+    twin = sp + 1 - 2 * (sp % 2)
+    peers = [((sp + 2 * k) % n, tp) for k in range(1, half)]
+    greet(peers + [(twin, tp)])
+    first, second = [None], []
+    for k in range(1, half):
+        copy = remote(
+            x_ref, out_ref.at[sp], send_sems.at[0, k], recv_sems.at[0, k], peers[k - 1]
+        )
+        copy.start()
+        first.append(copy)
+    for k in range(half):
+        s = (sp - 2 * k + n) % n
+        if k == 0:
+            src = x_ref
+        else:
+            first[k].wait_recv()
+            src = out_ref.at[s]
+        copy = remote(src, out_ref.at[s], send_sems.at[1, k], recv_sems.at[1, k], (twin, tp))
+        copy.start()
+        second.append(copy)
+        if k == 0:
+            out_ref[sp] = x_ref[...]
+    for copy in second:
+        copy.wait()
+    for copy in first[1:]:
+        copy.wait_send()
+
+
+def spread(x):
+    n = lax.axis_size("sp")
+    half = n // 2
+    return pl.pallas_call(
+        spread_kernel,
+        out_shape=jax.ShapeDtypeStruct((n,) + x.shape, x.dtype),
+        in_specs=[pl.BlockSpec(memory_space=pltpu.VMEM)],
+        out_specs=pl.BlockSpec(memory_space=pltpu.VMEM),
+        scratch_shapes=[pltpu.SemaphoreType.DMA((2, half)), pltpu.SemaphoreType.DMA((2, half))],
+        compiler_params=pltpu.CompilerParams(
+            collective_id=4, has_side_effects=True, vmem_limit_bytes=58 * 2**20
+        ),
+    )(x)
+
+
+def carried_in(x):
+    log_sum, mat, norm, top = x
+    heads, dim, _ = mat.shape
+    n, place = lax.axis_size("sp"), lax.axis_index("sp")
+    scalars = jnp.broadcast_to(jnp.concatenate([log_sum, top])[:, None], (2 * heads, dim))
+    packed = jnp.concatenate([mat.reshape(heads * dim, dim), norm, scalars], axis=0)
+    used = packed.shape[0]
+    packed = jnp.pad(packed, ((0, -used % 8), (0, 0)))
+    everything = spread(packed)
+    mats = everything[:, : heads * dim].reshape(n, heads, dim, dim)
+    norms = everything[:, heads * dim : heads * dim + heads]
+    logs = everything[:, heads * dim + heads : heads * dim + 2 * heads, 0]
+    tops = everything[:, heads * dim + 2 * heads : heads * dim + 3 * heads, 0]
+    index = jnp.arange(n)
+    reached = index < place
+    between = (index[None, :] > index[:, None]) & reached[None, :]
+    decay = jnp.sum(jnp.where(between[:, :, None], logs[None], 0.0), axis=1)
+    level = jnp.where(reached[:, None], tops + decay, lowest)
+    prior_max = jnp.max(level, axis=0)
+    scale = jnp.where(reached[:, None], jnp.exp(level - prior_max), 0.0)
+    prior_mat = jnp.sum(scale[:, :, None, None] * mats, axis=0)
+    prior_norm = jnp.sum(scale[:, :, None] * norms, axis=0)
+    return prior_mat, prior_norm, prior_max
 
 
 def block_pass(memory, inputs):
@@ -60,17 +282,6 @@
     return ((new_mat, new_norm, new_max), (numerator, denominator, row_max))
 
 
-def join_states(earlier, later):
-    early_log, early_mat, early_norm, early_max = earlier
-    late_log, late_mat, late_norm, late_max = later
-    joined_max = jnp.maximum(early_max + late_log, late_max)
-    early_scale = jnp.exp(early_max + late_log - joined_max)
-    late_scale = jnp.exp(late_max - joined_max)
-    joined_mat = early_scale[:, None, None] * early_mat + late_scale[:, None, None] * late_mat
-    joined_norm = early_scale[:, None] * early_norm + late_scale[:, None] * late_norm
-    return (early_log + late_log, joined_mat, joined_norm, joined_max)
-
-
 def matrix_memory_step(
     memory_queries,
     memory_keys,
@@ -118,9 +329,7 @@
     )
     numerator, denominator, row_max = (join_blocks(member) for member in pieces)
     running = jnp.cumsum(forget_log_value, axis=-1)
-    identity = (jnp.zeros((heads_here,), jnp.float32),) + empty_state
-    incoming = carried_in((running[:, -1],) + tuple(end_state), "sp", join_states, identity)
-    prior_mat, prior_norm, prior_max = incoming[1:]
+    prior_mat, prior_norm, prior_max = carried_in((running[:, -1],) + tuple(end_state))
     reached = running + prior_max[:, None]
     joined = jnp.maximum(row_max, reached)
     local_scale = jnp.exp(row_max - joined)
@@ -171,15 +380,14 @@
     partial_rows = jnp.einsum(
         "htd,hdc->tc", hidden, shaped, preferred_element_type=jnp.float32
     ).astype(jnp.bfloat16)
-    projected = lax.psum_scatter(
-        partial_rows.astype(jnp.float32).astype(jnp.bfloat16), "tp", scatter_dimension=0, tiled=True
-    ).astype(jnp.float32)
+    row_count, model_width = residual.shape
+    projected = collect(partial_rows.reshape(4, 4, row_count // 4, model_width), False)
+    projected = projected.reshape(row_count, model_width).astype(jnp.float32)
     mixed_rows = (residual.astype(jnp.float32) + projected).astype(jnp.bfloat16)
     mixed_wide = mixed_rows.astype(jnp.float32)
     norm_scale = lax.rsqrt(jnp.mean(mixed_wide * mixed_wide, axis=-1, keepdims=True) + epsilon)
     normed = (mixed_wide * norm_scale * expert_norm_gain).astype(jnp.bfloat16)
     sp_size = lax.axis_size("sp")
-    row_count, model_width = residual.shape
     top_count = routed_expert_index.shape[1]
     experts = sp_size * expert_gate_weight.shape[0]
     assigned = row_count * top_count
@@ -192,32 +400,14 @@
     padded = jnp.concatenate([normed, zero_row], axis=0)
     slot_table = jnp.full((experts * capacity,), row_count, jnp.int32)
     slot_table = slot_table.at[own_slots].set(jnp.arange(assigned, dtype=jnp.int32) // top_count)
-    arrived = lax.all_gather(
-        lax.all_to_all(
-            padded[slot_table.reshape(experts, 1, capacity)],
-            "sp",
-            split_axis=0,
-            concat_axis=0,
-            tiled=True,
-        ),
-        "tp",
-        axis=1,
-        tiled=True,
-    )
-    sources, owners, slot_span, width_in = arrived.shape
-    flat_rows = arrived.reshape(-1, width_in)
+    arrived = dispatch(padded[slot_table.reshape(experts, capacity)])
+    flat_rows = arrived.reshape(-1, model_width)
     gate_pre = jnp.dot(flat_rows, expert_gate_weight[0], preferred_element_type=jnp.float32)
     up_pre = jnp.dot(flat_rows, expert_up_weight[0], preferred_element_type=jnp.float32)
     hidden_act = (jax.nn.silu(gate_pre) * up_pre).astype(jnp.bfloat16)
     group_term = jnp.dot(hidden_act, expert_down_weight[0], preferred_element_type=jnp.float32)
     group_term = lax.optimization_barrier(group_term.astype(jnp.bfloat16)).astype(jnp.float32)
-    summed = lax.psum_scatter(
-        group_term.reshape(sources, owners, slot_span, width_in).astype(jnp.bfloat16),
-        "tp",
-        scatter_dimension=1,
-        tiled=True,
-    )
-    returned = lax.all_to_all(summed, "sp", split_axis=0, concat_axis=0, tiled=True)
+    returned = collect(group_term.astype(jnp.bfloat16).reshape(arrived.shape), True)
     picked = returned.reshape(experts * capacity, model_width)[own_slots]
     picked = picked.reshape(row_count, top_count, model_width).astype(jnp.float32)
     routed_sum = jnp.sum(picked * routed_expert_weight[:, :, None], axis=1)

time: 406 us -> 238 us (0.59)
  waiting for transfers between devices: 227 us -> 0.73 us
  Pallas kernels: 0 us -> 146 us
  blocking collectives: 76.3 us -> 0 us
  starting transfers between devices: 5.89 us -> 0.01 us
  other arithmetic: 22 us -> 16.9 us
    pallas_call x0 -> x4, Pallas kernels: none -> 146 us  [the longest x2 68.5 us: collect(): pl.pallas_call(functools.partial(collect_kernel, back), out_shape=jax.Sha...]
    unnamed x6 -> x1, waiting for transfers between devices: 102 us -> 0.71 us
    all_gather x2 -> x0, waiting for transfers between devices: 38.4 us -> none  [the longest x1 38.4 us: local(): lax.all_gather(lax.all_to_all(padded[slot_table.reshape(experts, 1, capac...]
    all_to_all x1 -> x0, blocking collectives: 36.6 us -> none  [local(): lax.all_to_all(padded[slot_table.reshape(experts, 1, capacity)], 'sp', sp...]
    all_to_all x1 -> x0, waiting for transfers between devices: 30.9 us -> none  [local(): lax.all_to_all(summed, 'sp', split_axis=0, concat_axis=0, tiled=True)]
    all_gather x1, waiting for transfers between devices: 29.1 us -> 0.02 us  [local(): weight_piece = lax.all_gather(cell_output_weight, 'sp', axis=1, tiled=True)]
    reduce_scatter x1 -> x0, waiting for transfers between devices: 26.4 us -> none  [local(): lax.psum_scatter(partial_rows.astype(jnp.float32).astype(jnp.bfloat16), '...]
    unnamed x1 -> x0, blocking collectives: 23.2 us -> none
  transfers between devices with their start and end apart: 6 -> 1, of which waited for: 5 -> 0; matrix products, arithmetic and copies ran while one was open for 4% -> 11% of each run, Pallas kernels for 0% -> 13%
where the time goes in v1:
time: 238 us; the launch traced here: 236 us
  Pallas kernels  146 us (61%)
  matrix products  39.1 us (16%)
  local copies, waits for them, and re-layouts  19.4 us (8%)
  other arithmetic  16.9 us (7%)
  between operations  13.8 us (6%)
    pallas_call x2, Pallas kernels, collect(): pl.pallas_call(functools.partial(collect_kernel, back), out_shape=jax.Sha...  68.5 us
    pallas_call x1, Pallas kernels, dispatch(): pl.pallas_call(dispatch_kernel, out_shape=jax.ShapeDtypeStruct((4, n, row...  47.1 us
    pallas_call x1, Pallas kernels, spread(): pl.pallas_call(spread_kernel, out_shape=jax.ShapeDtypeStruct((n,) + x.sha...  30.6 us
    dot_general x1, matrix products, local(): jnp.dot(hidden_act, expert_down_weight[0], preferred_element_type=jnp.flo...  17.6 us
    dot_general x1, matrix products, local(): jnp.dot(flat_rows, expert_gate_weight[0], preferred_element_type=jnp.floa...  9.99 us
    gather x1, local copies, waits for them, and re-layouts, local(): picked = returned.reshape(experts * capacity, model_width)[own_slots]  4.84 us
  transfers between devices with their start and end apart: 1, of which 0 were waited for; matrix products, arithmetic and copies ran while one was open for 11% of the time, Pallas kernels for 13%

profile of v1, /device:TPU:0, one launch (start us, length us, event | category | flops | bytes accessed | tf_op | source)
XLA Modules:
  0.0 236.2 jit_solution(987496611636118663)
XLA Ops:
  6.5 0.7 all-gather.2.cloned.1.call-update
  7.4 0.7 broadcast_multiply_fusion
  8.2 0.1 eq.29
  8.3 0.1 eq.25
  8.4 1.1 copy.72
  9.6 0.2 copy.73
  9.8 1.1 copy.70
  11.0 0.2 copy.71
  11.2 0.1 copy.68
  11.4 0.2 copy.69
  11.7 11.3 %while.21 = (s32[]{:T(128)}, f32[2,128,128]{2,1,0:T(8,128)S(1)}, f32[2,128]{1,0:T(2,128)S(1)}, f32[2]{0:T(128)S(1)}, f32[2,2,256,128]{3,2,0,1:T(8,128)S(1)}, /*i...) while((s32[]{:T(128)}, f32[2,128,128]{2,1,0:T(8,128)S(1)}, ...), condition=%wide.region_6.7_spmd.clone, body=%wide.region_0.6_spmd.clone.sunk | while | flops 607329536 | bytes 4625314 | solution.py:327
  11.7 0.6 reduce-window.38
  12.3 0.2 slice_reduce_fusion.6
  12.5 0.2 reduce-window.39
  12.8 0.2 slice_reduce_fusion.7
  12.9 0.2 fusion.113
  13.2 0.2 fusion.117
  13.5 0.6 fusion.118
  14.2 0.3 fusion.116
  14.5 0.3 fusion.119
  15.1 0.4 convolution_multiply_fusion.4
  15.4 1.1 fusion.120
  16.6 0.7 convolution_add_fusion.3
  17.4 0.6 reduce-window.38
  18.0 0.2 slice_reduce_fusion.6
  18.1 0.2 reduce-window.39
  18.4 0.2 slice_reduce_fusion.7
  18.6 0.2 fusion.113
  18.8 0.2 fusion.117
  19.1 0.6 fusion.118
  19.8 0.2 fusion.116
  20.2 0.3 fusion.119
  20.7 0.4 convolution_multiply_fusion.4
  21.1 1.0 fusion.120
  22.2 0.7 convolution_add_fusion.3
  23.0 0.6 reduce-window.22
  23.6 0.2 slice_reduce_fusion.3
  23.7 0.2 reduce-window.23
  24.4 0.7 pad.5.x_ref
  25.0 30.6 %shard_map.136 = f32[8,264,128]{2,1,0:T(8,128)} custom-call(f32[264,128]{1,0:T(8,128)} %pad.5.x_ref), custom_call_target="tpu_custom_call" | custom-call | tf_op jit(solution)/shard_map/pallas_call | solution.py:211
  55.7 0.8 fusion.62
  57.0 0.6 reduce-window.26
  57.6 0.2 slice_reduce_fusion.2
  58.0 0.1 mul.176
  58.2 1.4 scatter_custom_fusion
  59.7 0.8 exponential_select_fusion
  61.0 0.8 multiply_reduce_fusion.2
  62.0 1.6 multiply_reduce_fusion.1
  63.5 0.4 fusion.63
  64.0 0.2 bitcast_multiply_fusion.3
  64.2 1.2 fusion.40
  65.4 3.3 %bitcast_convert_fusion = bf16[512,2048]{1,0:T(8,128)(2,1)} fusion(bf16[2,512,128]{2,1,0:T(8,128)(2,1)S(1)} %fusion.40, bf16[2,128,2048]{2,1,0:T(8,128)(2,1)} %bitcast.266), kind=kOutput, calls=%fused_computation.63 | convolution fusion | flops 537919488 | bytes 3407872 | tf_op jit(solution)/shard_map/htd,hdc->tc/dot_general | solution.py:380
  68.7 18.2 %shard_map.137 = bf16[4,32,2048]{2,1,0:T(8,128)(2,1)} custom-call(bf16[4,4,32,2048]{3,2,1,0:T(8,128)(2,1)} %bitcast.256), custom_call_target="tpu_custom_call" | custom-call | tf_op jit(solution)/shard_map/pallas_call | solution.py:158
  87.0 1.3 fusion.41
  88.3 1.3 fusion.43
  89.6 3.2 %gather_fusion = bf16[320,2048]{1,0:T(8,128)(2,1)} fusion(bf16[129,2048]{1,0:T(8,128)(2,1)S(1)} %concatenate.11, s32[1024]{0:T(1024)S(1)} %pad_clamp_fusion.1), kind=kCustom, calls=%fused_computation | custom fusion | bytes 2622720 | tf_op jit(solution)/shard_map/gather | solution.py:403
  92.8 47.1 %shard_map.138 = bf16[4,8,40,2048]{3,2,1,0:T(8,128)(2,1)} custom-call(bf16[8,40,2048]{2,1,0:T(8,128)(2,1)} %bitcast.260), custom_call_target="tpu_custom_call" | custom-call | tf_op jit(solution)/shard_map/pallas_call | solution.py:91
  139.9 10.0 %fusion.36 = f32[1280,896]{1,0:T(8,128)} fusion(bf16[1280,2048]{1,0:T(8,128)(2,1)} %bitcast.257, bf16[1,2048,896]{2,1,0:T(8,128)(2,1)} %param.25), kind=kOutput, calls=%fused_computation.66 | convolution fusion | flops 4697620480 | bytes 13500416 | tf_op jit(solution)/shard_map/dot_general | solution.py:405
  149.9 17.6 %convolution_convert_fusion = bf16[1280,2048]{1,0:T(8,128)(2,1)} fusion(bf16[1,896,2048]{2,1,0:T(8,128)(2,1)} %param.27, f32[1280,896]{1,0:T(8,128)} %fusion.36, bf16[1280,2048]{1,0:T(8,128)(2,1)} %bitcast.258, bf16[1,2048,896]{2,1,0:T(8,128)(2,1)} %param.26), kind=kOutput, calls=%fused_computation.61 | convolution fusion | flops 9404743680 | bytes 22413312 | tf_op jit(solution)/shard_map/dot_general | solution.py:408
  167.4 50.3 %shard_map.139 = bf16[8,40,2048]{2,1,0:T(8,128)(2,1)} custom-call(bf16[4,8,40,2048]{3,2,1,0:T(8,128)(2,1)} %bitcast.259), custom_call_target="tpu_custom_call" | custom-call | tf_op jit(solution)/shard_map/pallas_call | solution.py:158
  217.7 4.8 %gather_fusion.1 = bf16[256,2048]{1,0:T(8,128)(2,1)} fusion(bf16[320,2048]{1,0:T(8,128)(2,1)} %bitcast.251, s32[1024]{0:T(1024)S(1)} %pad_clamp_fusion), kind=kCustom, calls=%fused_computation.1 | custom fusion | bytes 2098176 | tf_op jit(solution)/shard_map/gather | solution.py:411
  222.5 2.6 %reshape.532 = f32[128,2,2048]{2,1,0:T(2,128)S(1)} reshape(bf16[256,2048]{1,0:T(8,128)(2,1)} %gather_fusion.1) | data formatting | bytes 3145728 | tf_op jit(solution)/shard_map/convert_element_type | solution.py:412
  225.2 3.2 %multiply_reduce_fusion = f32[128,2048]{1,0:T(8,128)S(1)} fusion(f32[128,2,2048]{2,1,0:T(2,128)S(1)} %reshape.532, f32[128,2]{1,0:T(8,128)S(1)} %copy.88), kind=kLoop, calls=%fused_computation.68 | loop fusion | flops 786432 | bytes 3146752 | tf_op jit(solution)/shard_map/reduce_sum | solution.py:413
  228.4 1.0 fusion.44
  (91 shorter events, 3.6 us)
Async XLA Ops:
  6.5 4.6 %copy-start.2 = (bf16[512,256]{1,0:T(8,128)(2,1)S(1)}, bf16[512,256]{1,0:T(8,128)(2,1)}, u32[]{:S(2)}) copy-start(bf16[512,256]{1,0:T(8,128)(2,1)} %param.18) | copy-start | bytes 786436
  6.5 58.9 %all-gather.2.cloned.1.call-start = ((), (), s32[]{:S(2)}) async-start(), calls=%async_computation | async-start | bytes 1179648 | tf_op jit(solution)/shard_map/all_gather | solution.py:378
  7.3 4.3 %copy-start.5 = (f32[2,512]{1,0:T(2,128)S(1)}, f32[2,512]{1,0:T(2,128)}, u32[]{:S(2)}) copy-start(f32[2,512]{1,0:T(2,128)} %param.21) | copy-start | bytes 12292
  7.3 4.3 %copy-start.6 = (f32[2,512]{1,0:T(2,128)S(1)}, f32[2,512]{1,0:T(2,128)}, u32[]{:S(2)}) copy-start(f32[2,512]{1,0:T(2,128)} %param.20) | copy-start | bytes 12292
  7.3 4.3 %copy-start.3 = (f32[2,512]{1,0:T(2,128)S(1)}, f32[2,512]{1,0:T(2,128)}, u32[]{:S(2)}) copy-start(f32[2,512]{1,0:T(2,128)} %param.19) | copy-start | bytes 12292
  11.7 49.2 %copy-start.7 = (f32[128,2]{0,1:T(2,128)S(1)}, f32[128,2]{0,1:T(2,128)}, u32[]{:S(2)}) copy-start(f32[128,2]{0,1:T(2,128)} %param.29) | copy-start | bytes 3076
  64.2 22.8 %copy-start.1 = (bf16[128,2048]{1,0:T(8,128)(2,1)S(1)}, bf16[128,2048]{1,0:T(8,128)(2,1)}, u32[]{:S(2)}) copy-start(bf16[128,2048]{1,0:T(8,128)(2,1)} %param.22) | copy-start | bytes 1572868
  65.4 22.9 %copy-start.4 = (f32[2048]{0:T(1024)S(1)}, f32[2048]{0:T(1024)}, u32[]{:S(2)}) copy-start(f32[2048]{0:T(1024)} %param.24) | copy-start | bytes 24580
  222.5 5.8 %copy-start = (bf16[4,32,2048]{2,1,0:T(8,128)(2,1)S(1)}, bf16[4,32,2048]{2,1,0:T(8,128)(2,1)}, u32[]{:S(2)}) copy-start(bf16[4,32,2048]{2,1,0:T(8,128)(2,1)} %shard_map.137) | copy-start | bytes 1572868
Sparse Core Ops, SparseCore 0:
  9.4 48.4 all-gather.1

commit v2 on v1

--- a/solution.py
+++ b/solution.py
@@ -37,21 +37,22 @@
     )
 
 
+def far_first(n):
+    return sorted(range(1, n), key=lambda k: abs(2 * k - n))
+
+
 def dispatch_kernel(x_ref, out_ref, send_sems, recv_sems):
     sp, tp, n, p, q = places()
     peers = [((sp + k) % n, tp) for k in range(1, n)]
     greet(peers + [(sp, p), (sp, q)])
-    started, across = [], []
-    first = [None]
-    for k in range(1, n):
+    across, first, late = {}, {}, []
+    for k in far_first(n):
         copy = remote(
             x_ref.at[(sp + k) % n], out_ref.at[tp, sp],
             send_sems.at[0, k], recv_sems.at[0, k], peers[k - 1],
         )
         copy.start()
-        first.append(copy)
-    started += first[1:]
-    late = []
+        first[k] = copy
 
     def relay(k):
         across[k].wait_recv()
@@ -62,7 +63,8 @@
         copy.start()
         late.append(copy)
 
-    for k in range(n):
+    order = [0] + far_first(n)
+    for step, k in enumerate(order):
         s = (sp - k + n) % n
         if k == 0:
             src = x_ref.at[sp]
@@ -71,18 +73,18 @@
             src = out_ref.at[tp, s]
         copy = remote(src, out_ref.at[tp, s], send_sems.at[1, k], recv_sems.at[1, k], (sp, q))
         copy.start()
-        across.append(copy)
+        across[k] = copy
         copy = remote(src, out_ref.at[tp, s], send_sems.at[2, k], recv_sems.at[2, k], (sp, p))
         copy.start()
         late.append(copy)
         if k == 0:
             out_ref[tp, sp] = x_ref[sp]
         else:
-            relay(k - 1)
-    relay(n - 1)
+            relay(order[step - 1])
+    relay(order[-1])
     for copy in late:
         copy.wait()
-    for copy in started + across:
+    for copy in list(first.values()) + list(across.values()):
         copy.wait_send()
 
 
@@ -103,11 +105,12 @@
 def collect_kernel(back, x_ref, out_ref, near, sent, far, result, send_sems, recv_sems):
     sp, tp, n, p, q = places()
     chunks = x_ref.shape[1]
-    peers = [((sp + k) % n, tp) for k in range(1, n)] if back else []
+    offsets = far_first(n) + [0]
+    peers = [((sp + k) % n, tp) for k in offsets[:-1]] if back else []
     greet(peers + [(sp, p), (sp, q)])
 
     def at(k):
-        return (sp + 1 + k) % n if back else k
+        return (sp + offsets[k]) % n if back else k
 
     near_far, near_own, crossing, homeward = [], [], [], []
     for k in range(chunks):
@@ -295,9 +298,10 @@
     head_dim = channels // heads_here
 
     def heads_first(tensor):
-        return jnp.transpose(
-            tensor.astype(jnp.float32).reshape(tokens_here, heads_here, head_dim), (1, 0, 2)
-        )
+        pieces = [
+            tensor[:, head * head_dim : (head + 1) * head_dim] for head in range(heads_here)
+        ]
+        return jnp.stack(pieces).astype(jnp.float32)
 
     queries = heads_first(memory_queries) * head_dim ** (-0.5)
     forget_log_value = jax.nn.log_sigmoid(forget_gate_logits) + extra_log_decay

time: 238 us -> 237 us (level)
    pallas_call x1, Pallas kernels: 47.1 us -> 57.7 us  [dispatch(): pl.pallas_call(dispatch_kernel, out_shape=jax.ShapeDtypeStruct((4, n, row...]
    pallas_call x2, Pallas kernels: 68.5 us -> 61.8 us  [collect(): pl.pallas_call(functools.partial(collect_kernel, back), out_shape=jax.Sha...]
    pallas_call x1, Pallas kernels: 30.6 us -> 27.4 us  [spread(): pl.pallas_call(spread_kernel, out_shape=jax.ShapeDtypeStruct((n,) + x.sha...]
  transfers between devices with their start and end apart: 1 -> 1, of which waited for: 0 -> 0; matrix products, arithmetic and copies ran while one was open for 11% -> 12% of each run, Pallas kernels for 13% -> 12%
where the time goes in v2:
time: 237 us
  Pallas kernels  147 us (62%)
  matrix products  37.7 us (16%)
  other arithmetic  19.2 us (8%)
  local copies, waits for them, and re-layouts  18.2 us (8%)
  between operations  13.7 us (6%)
    pallas_call x2, Pallas kernels, collect(): pl.pallas_call(functools.partial(collect_kernel, back), out_shape=jax.Sha...  61.8 us
    pallas_call x1, Pallas kernels, dispatch(): pl.pallas_call(dispatch_kernel, out_shape=jax.ShapeDtypeStruct((4, n, row...  57.7 us
    pallas_call x1, Pallas kernels, spread(): pl.pallas_call(spread_kernel, out_shape=jax.ShapeDtypeStruct((n,) + x.sha...  27.4 us
    dot_general x1, matrix products, local(): jnp.dot(hidden_act, expert_down_weight[0], preferred_element_type=jnp.flo...  17.6 us
    dot_general x1, matrix products, local(): jnp.dot(flat_rows, expert_gate_weight[0], preferred_element_type=jnp.floa...  8.89 us
    reduce_sum x1, other arithmetic, local(): routed_sum = jnp.sum(picked * routed_expert_weight[:, :, None], axis=1)  4.81 us
  transfers between devices with their start and end apart: 1, of which 0 were waited for; matrix products, arithmetic and copies ran while one was open for 12% of the time, Pallas kernels for 12%

profile of v2, /device:TPU:0, one launch (start us, length us, event | category | flops | bytes accessed | tf_op | source)
XLA Modules:
  0.0 236.6 jit_solution(5220659672933719756)
XLA Ops:
  6.5 0.7 all-gather.2.cloned.1.call-update
  7.3 0.7 broadcast_multiply_fusion
  8.1 0.1 eq.29
  8.3 0.1 eq.25
  8.4 1.0 slice_bitcast_fusion.1
  9.5 1.0 fusion.71
  10.4 1.0 fusion.70
  11.4 0.7 fusion.53
  12.3 11.3 %while.21 = (s32[]{:T(128)}, f32[2,128,128]{2,1,0:T(8,128)S(1)}, f32[2,128]{1,0:T(2,128)S(1)}, f32[2]{0:T(128)S(1)}, f32[2,2,256,128]{3,2,0,1:T(8,128)S(1)}, /*i...) while((s32[]{:T(128)}, f32[2,128,128]{2,1,0:T(8,128)S(1)}, ...), condition=%wide.region_6.7_spmd.clone, body=%wide.region_0.6_spmd.clone.sunk | while | flops 607329536 | bytes 4625314 | solution.py:331
  12.4 0.6 reduce-window.38
  13.0 0.2 slice_reduce_fusion.6
  13.2 0.2 reduce-window.39
  13.4 0.2 slice_reduce_fusion.7
  13.6 0.2 fusion.119
  13.8 0.2 fusion.123
  14.1 0.6 fusion.124
  14.9 0.3 fusion.122
  15.2 0.3 fusion.125
  15.7 0.4 convolution_multiply_fusion.4
  16.1 1.0 fusion.126
  17.2 0.7 convolution_add_fusion.3
  18.0 0.6 reduce-window.38
  18.6 0.2 slice_reduce_fusion.6
  18.8 0.2 reduce-window.39
  19.1 0.2 slice_reduce_fusion.7
  19.2 0.2 fusion.119
  19.5 0.2 fusion.123
  19.8 0.6 fusion.124
  20.5 0.2 fusion.122
  20.8 0.3 fusion.125
  21.4 0.4 convolution_multiply_fusion.4
  21.8 1.0 fusion.126
  22.9 0.7 convolution_add_fusion.3
  23.6 0.6 reduce-window.22
  24.2 0.2 slice_reduce_fusion.3
  24.4 0.2 reduce-window.23
  25.0 0.7 pad.5.x_ref
  25.7 27.4 %shard_map.136 = f32[8,264,128]{2,1,0:T(8,128)} custom-call(f32[264,128]{1,0:T(8,128)} %pad.5.x_ref), custom_call_target="tpu_custom_call" | custom-call | tf_op jit(solution)/shard_map/pallas_call | solution.py:214
  53.1 0.8 fusion.69
  54.2 0.1 fusion.61
  54.4 0.6 reduce-window.26
  55.0 0.2 slice_reduce_fusion.2
  55.4 0.1 mul.175
  55.6 1.4 scatter_custom_fusion
  57.1 0.8 exponential_select_fusion
  58.4 0.8 multiply_reduce_fusion.2
  59.4 1.6 multiply_reduce_fusion.1
  60.9 0.5 fusion.46
  61.5 0.1 subtract_exponential_fusion.3
  61.6 0.2 bitcast_multiply_fusion.3
  61.8 0.7 fusion.40
  62.5 3.3 %bitcast_convert_fusion = bf16[512,2048]{1,0:T(8,128)(2,1)} fusion(bf16[2,512,128]{2,1,0:T(8,128)(2,1)S(1)} %fusion.40, bf16[2,128,2048]{2,1,0:T(8,128)(2,1)} %bitcast.250), kind=kOutput, calls=%fused_computation.63 | convolution fusion | flops 537919488 | bytes 3407872 | tf_op jit(solution)/shard_map/htd,hdc->tc/dot_general | solution.py:384
  65.9 18.2 %shard_map.137 = bf16[4,32,2048]{2,1,0:T(8,128)(2,1)} custom-call(bf16[4,4,32,2048]{3,2,1,0:T(8,128)(2,1)} %bitcast.245), custom_call_target="tpu_custom_call" | custom-call | tf_op jit(solution)/shard_map/pallas_call | solution.py:161
  84.1 1.3 fusion.41
  85.4 1.3 fusion.43
  86.7 3.2 %gather_fusion = bf16[320,2048]{1,0:T(8,128)(2,1)} fusion(bf16[129,2048]{1,0:T(8,128)(2,1)S(1)} %concatenate.14, s32[1024]{0:T(1024)S(1)} %pad_clamp_fusion.1), kind=kCustom, calls=%fused_computation | custom fusion | bytes 2622720 | tf_op jit(solution)/shard_map/gather | solution.py:407
  89.9 57.7 %shard_map.138 = bf16[4,8,40,2048]{3,2,1,0:T(8,128)(2,1)} custom-call(bf16[8,40,2048]{2,1,0:T(8,128)(2,1)} %bitcast.249), custom_call_target="tpu_custom_call" | custom-call | tf_op jit(solution)/shard_map/pallas_call | solution.py:93
  147.7 8.9 %fusion.36 = f32[1280,896]{1,0:T(8,128)} fusion(bf16[1280,2048]{1,0:T(8,128)(2,1)} %bitcast.246, bf16[1,2048,896]{2,1,0:T(8,128)(2,1)S(1)} %copy-done.5), kind=kOutput, calls=%fused_computation.66 | convolution fusion | flops 4697620480 | bytes 13500416 | tf_op jit(solution)/shard_map/dot_general | solution.py:409
  156.6 17.6 %convolution_convert_fusion = bf16[1280,2048]{1,0:T(8,128)(2,1)} fusion(bf16[1,896,2048]{2,1,0:T(8,128)(2,1)} %param.27, f32[1280,896]{1,0:T(8,128)} %fusion.36, bf16[1280,2048]{1,0:T(8,128)(2,1)} %bitcast.247, bf16[1,2048,896]{2,1,0:T(8,128)(2,1)} %param.26), kind=kOutput, calls=%fused_computation.61 | convolution fusion | flops 9404743680 | bytes 22413312 | tf_op jit(solution)/shard_map/dot_general | solution.py:412
  174.1 43.5 %shard_map.139 = bf16[8,40,2048]{2,1,0:T(8,128)(2,1)} custom-call(bf16[4,8,40,2048]{3,2,1,0:T(8,128)(2,1)} %bitcast.248), custom_call_target="tpu_custom_call" | custom-call | tf_op jit(solution)/shard_map/pallas_call | solution.py:161
  217.7 3.8 %gather_fusion.1 = bf16[256,2048]{1,0:T(8,128)(2,1)S(1)} fusion(bf16[320,2048]{1,0:T(8,128)(2,1)} %bitcast.243, s32[1024]{0:T(1024)S(1)} %pad_clamp_fusion), kind=kCustom, calls=%fused_computation.1 | custom fusion | bytes 2098176 | tf_op jit(solution)/shard_map/gather | solution.py:415
  221.5 2.4 %reshape.520 = f32[128,2,2048]{2,1,0:T(2,128)} reshape(bf16[256,2048]{1,0:T(8,128)(2,1)S(1)} %gather_fusion.1) | data formatting | bytes 3145728 | tf_op jit(solution)/shard_map/convert_element_type | solution.py:416
  223.9 4.8 %multiply_reduce_fusion = f32[128,2048]{1,0:T(8,128)S(1)} fusion(f32[128,2,2048]{2,1,0:T(2,128)} %reshape.520, f32[128,2]{1,0:T(8,128)S(1)} %copy.53), kind=kLoop, calls=%fused_computation.68 | loop fusion | flops 786432 | bytes 3146752 | tf_op jit(solution)/shard_map/reduce_sum | solution.py:417
  228.7 1.0 fusion.44
  (83 shorter events, 3.3 us)
Async XLA Ops:
  6.5 5.8 %copy-start.2 = (f32[2,512]{1,0:T(2,128)S(1)}, f32[2,512]{1,0:T(2,128)}, u32[]{:S(2)}) copy-start(f32[2,512]{1,0:T(2,128)} %param.19) | copy-start | bytes 12292
  6.5 56.0 %all-gather.2.cloned.1.call-start = ((), (), s32[]{:S(2)}) async-start(), calls=%async_computation | async-start | bytes 1179648 | tf_op jit(solution)/shard_map/all_gather | solution.py:382
  12.3 45.9 %copy-start.4 = (f32[128,2]{0,1:T(2,128)S(1)}, f32[128,2]{0,1:T(2,128)}, u32[]{:S(2)}) copy-start(f32[128,2]{0,1:T(2,128)} %param.29) | copy-start | bytes 3076
  62.5 21.6 %copy-start.1 = (bf16[128,2048]{1,0:T(8,128)(2,1)S(1)}, bf16[128,2048]{1,0:T(8,128)(2,1)}, u32[]{:S(2)}) copy-start(bf16[128,2048]{1,0:T(8,128)(2,1)} %param.22) | copy-start | bytes 1572868
  62.5 22.9 %copy-start.3 = (f32[2048]{0:T(1024)S(1)}, f32[2048]{0:T(1024)}, u32[]{:S(2)}) copy-start(f32[2048]{0:T(1024)} %param.24) | copy-start | bytes 24580
  89.9 57.7 %copy-start.5 = (bf16[1,2048,896]{2,1,0:T(8,128)(2,1)S(1)}, bf16[1,2048,896]{2,1,0:T(8,128)(2,1)}, u32[]{:S(2)}) copy-start(bf16[1,2048,896]{2,1,0:T(8,128)(2,1)} %param.25) | copy-start | bytes 11010052
  221.5 7.2 %copy-start = (bf16[4,32,2048]{2,1,0:T(8,128)(2,1)S(1)}, bf16[4,32,2048]{2,1,0:T(8,128)(2,1)}, u32[]{:S(2)}) copy-start(bf16[4,32,2048]{2,1,0:T(8,128)(2,1)} %shard_map.137) | copy-start | bytes 1572868
Sparse Core Ops, SparseCore 0:
  9.4 47.1 all-gather.1

commit v3 on v2

--- a/solution.py
+++ b/solution.py
@@ -400,11 +400,13 @@
         routed_expert_index, lax.axis_index("tp") * row_count, row_count, 0
     )
     own_slots = slot_index(own_ids, experts, capacity)
-    zero_row = jnp.zeros((1, model_width), jnp.bfloat16)
-    padded = jnp.concatenate([normed, zero_row], axis=0)
-    slot_table = jnp.full((experts * capacity,), row_count, jnp.int32)
-    slot_table = slot_table.at[own_slots].set(jnp.arange(assigned, dtype=jnp.int32) // top_count)
-    arrived = dispatch(padded[slot_table.reshape(experts, capacity)])
+    slots = own_slots.reshape(row_count, top_count)
+    at_slot = slots[:, :, None] == jnp.arange(experts * capacity, dtype=jnp.int32)
+    chosen = jnp.any(at_slot, axis=1).astype(jnp.bfloat16)
+    outgoing = lax.dot_general(
+        chosen, normed, (((0,), (0,)), ((), ())), preferred_element_type=jnp.float32
+    ).astype(jnp.bfloat16)
+    arrived = dispatch(outgoing.reshape(experts, capacity, model_width))
     flat_rows = arrived.reshape(-1, model_width)
     gate_pre = jnp.dot(flat_rows, expert_gate_weight[0], preferred_element_type=jnp.float32)
     up_pre = jnp.dot(flat_rows, expert_up_weight[0], preferred_element_type=jnp.float32)
@@ -412,9 +414,12 @@
     group_term = jnp.dot(hidden_act, expert_down_weight[0], preferred_element_type=jnp.float32)
     group_term = lax.optimization_barrier(group_term.astype(jnp.bfloat16)).astype(jnp.float32)
     returned = collect(group_term.astype(jnp.bfloat16).reshape(arrived.shape), True)
-    picked = returned.reshape(experts * capacity, model_width)[own_slots]
-    picked = picked.reshape(row_count, top_count, model_width).astype(jnp.float32)
-    routed_sum = jnp.sum(picked * routed_expert_weight[:, :, None], axis=1)
+    share = jnp.sum(jnp.where(at_slot, routed_expert_weight[:, :, None], 0.0), axis=1)
+    routed_sum = jnp.dot(
+        share,
+        returned.reshape(experts * capacity, model_width).astype(jnp.float32),
+        precision=highest,
+    )
     return (mixed_wide + routed_sum).astype(jnp.bfloat16)
 
 

time: 237 us -> 222 us (0.937)
  local copies, waits for them, and re-layouts: 18.2 us -> 7.03 us
  other arithmetic: 19.2 us -> 11.5 us
  matrix products: 37.7 us -> 42.7 us
    gather x2 -> x0, local copies, waits for them, and re-layouts: 7.05 us -> none  [the longest x1 3.85 us: local(): picked = returned.reshape(experts * capacity, model_width)[own_slots]]
    dot_general x0 -> x2, matrix products: none -> 4.84 us  [the longest x1 3.16 us: local(): jnp.dot(share, returned.reshape(experts * capacity, model_width).astype(j...]
    reduce_sum x1, other arithmetic: 4.81 us -> 0.04 us  [local(): jnp.sum(jnp.where(at_slot, routed_expert_weight[:, :, None], 0.0), axis=1)]
    pallas_call x1, Pallas kernels: 57.7 us -> 54.6 us  [dispatch(): pl.pallas_call(dispatch_kernel, out_shape=jax.ShapeDtypeStruct((4, n, row...]
  transfers between devices with their start and end apart: 1 -> 1, of which waited for: 0 -> 0; matrix products, arithmetic and copies ran while one was open for 12% -> 11% of each run, Pallas kernels for 12% -> 13%
where the time goes in v3:
time: 222 us; the launch traced here: 221 us
  Pallas kernels  145 us (65%)
  matrix products  42.7 us (19%)
  between operations  13.7 us (6%)
  other arithmetic  11.5 us (5%)
  local copies, waits for them, and re-layouts  7.03 us (3%)
    pallas_call x2, Pallas kernels, collect(): pl.pallas_call(functools.partial(collect_kernel, back), out_shape=jax.Sha...  61.8 us
    pallas_call x1, Pallas kernels, dispatch(): pl.pallas_call(dispatch_kernel, out_shape=jax.ShapeDtypeStruct((4, n, row...  54.6 us
    pallas_call x1, Pallas kernels, spread(): pl.pallas_call(spread_kernel, out_shape=jax.ShapeDtypeStruct((n,) + x.sha...  28.9 us
    dot_general x1, matrix products, local(): jnp.dot(hidden_act, expert_down_weight[0], preferred_element_type=jnp.flo...  17.6 us
    dot_general x1, matrix products, local(): jnp.dot(flat_rows, expert_gate_weight[0], preferred_element_type=jnp.floa...  8.91 us
  transfers between devices with their start and end apart: 1, of which 0 were waited for; matrix products, arithmetic and copies ran while one was open for 11% of the time, Pallas kernels for 13%

profile of v3, /device:TPU:0, one launch (start us, length us, event | category | flops | bytes accessed | tf_op | source)
XLA Modules:
  0.0 221.2 jit_solution(4119506276037118616)
XLA Ops:
  6.5 0.7 all-gather.2.cloned.1.call-update
  7.3 0.1 copy.62
  7.5 0.1 eq.42
  7.6 0.1 eq.38
  7.7 1.0 slice_bitcast_fusion.1
  8.8 1.0 fusion.74
  9.8 1.0 fusion.73
  10.8 0.7 fusion.57
  11.7 11.3 %while.21 = (s32[]{:T(128)}, f32[2,128,128]{2,1,0:T(8,128)S(1)}, f32[2,128]{1,0:T(2,128)S(1)}, f32[2]{0:T(128)S(1)}, f32[2,2,256,128]{3,2,0,1:T(8,128)S(1)}, /*i...) while((s32[]{:T(128)}, f32[2,128,128]{2,1,0:T(8,128)S(1)}, ...), condition=%wide.region_6.7_spmd.clone, body=%wide.region_0.6_spmd.clone.sunk | while | flops 607329536 | bytes 4625314 | solution.py:331
  11.7 0.6 reduce-window.38
  12.3 0.2 slice_reduce_fusion.6
  12.5 0.2 reduce-window.39
  12.8 0.2 slice_reduce_fusion.7
  12.9 0.2 fusion.125
  13.2 0.2 fusion.129
  13.5 0.6 fusion.130
  14.2 0.3 fusion.128
  14.5 0.3 fusion.131
  14.9 0.1 broadcast_add_fusion.2
  15.1 0.4 convolution_multiply_fusion.4
  15.5 1.1 fusion.132
  16.6 0.7 convolution_add_fusion.4
  17.4 0.6 reduce-window.38
  18.0 0.2 slice_reduce_fusion.6
  18.2 0.2 reduce-window.39
  18.4 0.2 slice_reduce_fusion.7
  18.6 0.2 fusion.125
  18.8 0.2 fusion.129
  19.1 0.6 fusion.130
  19.9 0.2 fusion.128
  20.2 0.3 fusion.131
  20.6 0.1 bitcast_dynamic-update-slice_fusion.2
  20.7 0.4 convolution_multiply_fusion.4
  21.1 1.1 fusion.132
  22.3 0.7 convolution_add_fusion.4
  23.0 0.6 reduce-window.22
  23.6 0.2 slice_reduce_fusion.3
  23.8 0.2 reduce-window.23
  24.1 0.1 copy.61
  24.3 0.1 maximum_maximum_fusion
  24.4 0.7 pad.4.x_ref
  25.1 28.9 %shard_map.136 = f32[8,264,128]{2,1,0:T(8,128)} custom-call(f32[264,128]{1,0:T(8,128)} %pad.4.x_ref), custom_call_target="tpu_custom_call" | custom-call | tf_op jit(solution)/shard_map/pallas_call | solution.py:214
  54.0 0.8 fusion.72
  54.9 0.1 copy.44
  55.1 0.1 fusion.63
  55.4 0.8 exponential_select_fusion
  56.4 0.6 reduce-window.26
  57.0 0.2 slice_reduce_fusion.2
  57.3 0.1 reduce_sum.75
  57.5 0.8 multiply_reduce_fusion.1
  58.7 1.6 multiply_reduce_fusion
  60.2 0.5 fusion.49
  60.7 0.1 subtract_exponential_fusion.3
  60.9 0.2 bitcast_multiply_fusion.3
  61.1 0.7 fusion.41
  61.8 3.4 %bitcast_convert_fusion = bf16[512,2048]{1,0:T(8,128)(2,1)} fusion(bf16[2,512,128]{2,1,0:T(8,128)(2,1)S(1)} %fusion.41, bf16[2,128,2048]{2,1,0:T(8,128)(2,1)} %bitcast.244), kind=kOutput, calls=%fused_computation.60 | convolution fusion | flops 537919488 | bytes 3407872 | tf_op jit(solution)/shard_map/htd,hdc->tc/dot_general | solution.py:384
  65.2 18.2 %shard_map.137 = bf16[4,32,2048]{2,1,0:T(8,128)(2,1)} custom-call(bf16[4,4,32,2048]{3,2,1,0:T(8,128)(2,1)} %bitcast.238), custom_call_target="tpu_custom_call" | custom-call | tf_op jit(solution)/shard_map/pallas_call | solution.py:161
  83.4 1.3 fusion.42
  84.8 1.7 convolution_convert_fusion.1
  86.5 54.6 %shard_map.138 = bf16[4,8,40,2048]{3,2,1,0:T(8,128)(2,1)} custom-call(bf16[8,40,2048]{2,1,0:T(8,128)(2,1)} %bitcast.243), custom_call_target="tpu_custom_call" | custom-call | tf_op jit(solution)/shard_map/pallas_call | solution.py:93
  141.1 8.9 %fusion.36 = f32[1280,896]{1,0:T(8,128)} fusion(bf16[1280,2048]{1,0:T(8,128)(2,1)} %bitcast.239, bf16[1,2048,896]{2,1,0:T(8,128)(2,1)S(1)} %copy-done.5), kind=kOutput, calls=%fused_computation.63 | convolution fusion | flops 4697620480 | bytes 13500416 | tf_op jit(solution)/shard_map/dot_general | solution.py:411
  150.0 17.6 %convolution_convert_fusion = bf16[1280,2048]{1,0:T(8,128)(2,1)} fusion(bf16[1,896,2048]{2,1,0:T(8,128)(2,1)} %param.27, f32[1280,896]{1,0:T(8,128)} %fusion.36, bf16[1280,2048]{1,0:T(8,128)(2,1)} %bitcast.240, bf16[1,2048,896]{2,1,0:T(8,128)(2,1)} %param.26), kind=kOutput, calls=%fused_computation.58 | convolution fusion | flops 9404743680 | bytes 22413312 | tf_op jit(solution)/shard_map/dot_general | solution.py:414
  167.6 43.6 %shard_map.139 = bf16[8,40,2048]{2,1,0:T(8,128)(2,1)} custom-call(bf16[4,8,40,2048]{3,2,1,0:T(8,128)(2,1)} %bitcast.241), custom_call_target="tpu_custom_call" | custom-call | tf_op jit(solution)/shard_map/pallas_call | solution.py:161
  211.2 3.2 %fusion.38 = bf16[128,2048]{1,0:T(8,128)(2,1)} fusion(f32[128,320]{0,1:T(8,128)S(1)} %select_reduce_fusion, bf16[320,2048]{1,0:T(8,128)(2,1)} %bitcast.242, bf16[128,2048]{1,0:T(8,128)(2,1)S(1)} %get-tuple-element.153), kind=kOutput, calls=%fused_computation.67 | convolution fusion | flops 1007419392 | bytes 2523136 | tf_op jit(solution)/shard_map/dot_general | solution.py:418
  (72 shorter events, 2.4 us)
Async XLA Ops:
  6.5 0.8 copy-start
  6.5 5.1 %copy-start.2 = (f32[2,512]{1,0:T(2,128)S(1)}, f32[2,512]{1,0:T(2,128)}, u32[]{:S(2)}) copy-start(f32[2,512]{1,0:T(2,128)} %param.19) | copy-start | bytes 12292
  6.5 55.3 %all-gather.2.cloned.1.call-start = ((), (), s32[]{:S(2)}) async-start(), calls=%async_computation | async-start | bytes 1179648 | tf_op jit(solution)/shard_map/all_gather | solution.py:382
  11.7 46.8 %copy-start.4 = (f32[128,2]{0,1:T(2,128)S(1)}, f32[128,2]{0,1:T(2,128)}, u32[]{:S(2)}) copy-start(f32[128,2]{0,1:T(2,128)} %param.29) | copy-start | bytes 3076
  61.8 21.7 %copy-start.1 = (bf16[128,2048]{1,0:T(8,128)(2,1)S(1)}, bf16[128,2048]{1,0:T(8,128)(2,1)}, u32[]{:S(2)}) copy-start(bf16[128,2048]{1,0:T(8,128)(2,1)} %param.22) | copy-start | bytes 1572868
  61.8 23.0 %copy-start.3 = (f32[2048]{0:T(1024)S(1)}, f32[2048]{0:T(1024)}, u32[]{:S(2)}) copy-start(f32[2048]{0:T(1024)} %param.24) | copy-start | bytes 24580
  86.5 54.6 %copy-start.5 = (bf16[1,2048,896]{2,1,0:T(8,128)(2,1)S(1)}, bf16[1,2048,896]{2,1,0:T(8,128)(2,1)}, u32[]{:S(2)}) copy-start(bf16[1,2048,896]{2,1,0:T(8,128)(2,1)} %param.25) | copy-start | bytes 11010052
Sparse Core Ops, SparseCore 0:
  9.4 45.7 all-gather.1
